TPU v7x, 512 devices: a whole 4x4x16 slice. The times are simulated.
512 devices in a mesh: sp: 64 (over z, y), tp: 8 (over x, core).
Axes of the slice: x: 4, y: 4, z: 16, core: 2. Of those that a mesh axis runs over, the one named last changes fastest.
Arguments:
- prompt: bfloat16 [2, 12288, 4096], P(None, 'sp'), as said below
- w_key: bfloat16 [4096, 2048], P('sp', 'tp'), may hold values from -0.09375 to 0.09375
- w_value: bfloat16 [4096, 4096], P('sp', 'tp'), may hold values from -0.09375 to 0.09375
- w_igate: bfloat16 [4096, 8], replicated, may hold values from -0.09375 to 0.09375
- w_fgate: bfloat16 [4096, 8], replicated, may hold values from -0.09375 to 0.09375
- input_bias: float32 [8], replicated, may hold values from -1 to 120
- forget_bias: float32 [8], replicated, may hold values from 4 to 20
- new_query: bfloat16 [2, 8, 256], P(None, 'tp'), may hold values from -6 to 6
- new_key: bfloat16 [2, 8, 256], P(None, 'tp'), may hold values from -6 to 6
- new_value: bfloat16 [2, 8, 512], P(None, 'tp'), may hold values from -6 to 6
- new_gates: float32 [2, 2, 8], P(None, None, 'tp'), may hold values from 2 to 9
Outputs:
- cache_memory: bfloat16 [2, 8, 256, 512], P(None, 'tp', 'sp')
- cache_norm: float32 [2, 8, 256], P(None, 'tp', 'sp')
- cache_max: float32 [2, 8], P(None, 'tp')
- first_read: bfloat16 [2, 8, 512], P(None, 'tp')
Inputs may be any that keep to these rules, and one draw needn't show every extreme that they name: `prompt`: Real-valued features, each entry drawn independently; their magnitude differs from one block of 192 positions to the next.
All inputs are finite; a program needn't handle non-finite values.
Results may differ from a plain program's by a relative error of at most 0.019.
Values may be sent and summed in bfloat16 or wider, within the bound.
A program may use at most 64 MiB of HBM per device.

v0:
```python
import jax
import jax.numpy as jnp
from jax import lax
from jax.sharding import PartitionSpec as P


def in_one_piece(arrays, axis, dim, along):
    ends, at = ([], 0)
    for a in arrays[:-1]:
        at += a.shape[along]
        ends.append(at)
    both = jnp.concatenate(arrays, axis=along)
    return tuple(jnp.split(lax.all_gather(both, axis, axis=dim, tiled=True), ends, axis=along))


def in_blocks(value, dim, devices):
    shape = value.shape
    blocks = value.reshape(*shape[:dim], devices, shape[dim] // devices, *shape[dim + 1 :])
    return jnp.moveaxis(blocks, dim, 0)


def summed_on_arrival(value, axis, dim):
    blocks = in_blocks(value, dim, lax.axis_size(axis))
    arrived = lax.all_to_all(blocks, axis, split_axis=0, concat_axis=0, tiled=True)
    return arrived.astype(jnp.float32).sum(axis=0)


def summed_on_arrival_2(value, axis, dim):
    devices = lax.axis_size(axis)
    blocks = lax.all_to_all(in_blocks(value, dim, devices), axis, 0, 0, tiled=True)
    return jnp.sum(blocks, axis=0)


def copy_for_each(value, axis):
    copies = jnp.broadcast_to(value, (lax.axis_size(axis), *value.shape))
    return lax.all_to_all(copies, axis, split_axis=0, concat_axis=0, tiled=True)


def over_copies(value, axis):
    return copy_for_each(value, axis).sum(axis=0)


def together(arrays, axis):
    ends = [0]
    for a in arrays:
        ends.append(ends[-1] + a.size)
    so_far = over_copies(jnp.concatenate([a.ravel() for a in arrays]), axis)
    return tuple((so_far[b:e].reshape(a.shape) for a, b, e in zip(arrays, ends, ends[1:])))


def per_device(
    prompt,
    w_key,
    w_value,
    w_igate,
    w_fgate,
    input_bias,
    forget_bias,
    new_query,
    new_key,
    new_value,
    new_gates,
):
    seq_count, span_len, model_width = prompt.shape
    local_heads = new_query.shape[1]
    key_size = new_query.shape[2]
    value_size = new_value.shape[2]
    key_scale = key_size ** (-0.5)
    token_rows = prompt.reshape(seq_count * span_len, model_width)
    whole_key, whole_value = in_one_piece((w_key, w_value), "sp", 0, 1)
    key_rows = jnp.dot(token_rows, whole_key, preferred_element_type=jnp.float32).astype(
        jnp.bfloat16
    )
    value_rows = jnp.dot(token_rows, whole_value, preferred_element_type=jnp.float32).astype(
        jnp.bfloat16
    )
    head_start = lax.axis_index("tp") * local_heads
    input_all = jnp.dot(token_rows, w_igate, preferred_element_type=jnp.float32) + input_bias
    forget_all = jnp.dot(token_rows, w_fgate, preferred_element_type=jnp.float32) + forget_bias
    input_gate = lax.dynamic_slice_in_dim(input_all, head_start, local_heads, 1).reshape(
        seq_count, span_len, local_heads
    )
    log_forget = jax.nn.log_sigmoid(
        lax.dynamic_slice_in_dim(forget_all, head_start, local_heads, 1)
    ).reshape(seq_count, span_len, local_heads)
    block_total = jnp.sum(log_forget, axis=1)
    forget_after = block_total[:, None] - jnp.cumsum(log_forget, axis=1)
    log_weight = forget_after + input_gate
    block_max = jnp.max(log_weight, axis=1)
    key_blocks = key_rows.reshape(seq_count, span_len, local_heads, key_size).astype(jnp.float32)
    decayed = (jnp.exp(log_weight - block_max[:, None])[..., None] * key_scale * key_blocks).astype(
        jnp.bfloat16
    )
    value_blocks = value_rows.reshape(seq_count, span_len, local_heads, value_size)
    block_norm = jnp.sum(decayed.astype(jnp.float32), axis=1)
    every_total, every_max = (
        lax.all_gather(block_total[None], "sp", axis=0, tiled=True),
        lax.all_gather(block_max[None], "sp", axis=0, tiled=True),
    )
    later_all = jnp.flip(jnp.cumsum(jnp.flip(every_total, 0), axis=0), 0) - every_total
    lift_all = later_all + every_max
    global_max = jnp.max(lift_all, axis=0)
    own_mask = jnp.arange(every_total.shape[0]) == lax.axis_index("sp")
    block_lift = jnp.sum(jnp.where(own_mask[:, None, None], lift_all, 0.0), axis=0)
    factor = jnp.exp(block_lift - global_max)
    scaled_norm = factor[:, :, None] * block_norm
    query_full = new_query.astype(jnp.float32)
    piece = jnp.einsum("sthk,sthv->kshv", decayed, value_blocks, preferred_element_type=jnp.float32)
    owned = summed_on_arrival((factor[None, :, :, None] * piece).astype(jnp.bfloat16), "sp", 0)
    memory_rows = jnp.transpose(owned, (1, 2, 0, 3))
    norm_rows = summed_on_arrival_2(scaled_norm, "sp", 2)
    token_score = jnp.einsum(
        "shk,sthk->sth", new_query, decayed, preferred_element_type=jnp.float32
    )
    score_high = token_score.astype(jnp.bfloat16)
    score_low = (token_score - score_high.astype(jnp.float32)).astype(jnp.bfloat16)
    weighted = jnp.einsum(
        "sth,sthv->shv", score_high, value_blocks, preferred_element_type=jnp.float32
    )
    weighted = weighted + jnp.einsum(
        "sth,sthv->shv", score_low, value_blocks, preferred_element_type=jnp.float32
    )
    partial_state = factor[..., None] * weighted
    partial_norm = jnp.sum(query_full * scaled_norm, axis=-1)
    query_state, query_norm = together((partial_state, partial_norm), "sp")
    forget_new = jax.nn.log_sigmoid(new_gates[1])
    input_new = new_gates[0]
    mixed = jnp.maximum(forget_new + global_max, input_new)
    carried = jnp.exp(forget_new + global_max - mixed)
    fresh = jnp.exp(input_new - mixed)
    own_score = jnp.sum(query_full * new_key.astype(jnp.float32), axis=-1) * key_scale
    numer = carried[..., None] * query_state + (fresh * own_score)[..., None] * new_value.astype(
        jnp.float32
    )
    denom = carried * query_norm + fresh * own_score
    first_read = (numer / jnp.maximum(jnp.abs(denom), 1.0)[..., None]).astype(jnp.bfloat16)
    return (memory_rows.astype(jnp.bfloat16), norm_rows, global_max, first_read)


def solution(mesh):
    placed = (
        P(None, "sp", None),
        P("sp", "tp"),
        P("sp", "tp"),
        P(),
        P(),
        P(),
        P(),
        P(None, "tp", None),
        P(None, "tp", None),
        P(None, "tp", None),
        P(None, None, "tp"),
    )
    return jax.shard_map(
        per_device,
        mesh=mesh,
        in_specs=placed,
        out_specs=(
            P(None, "tp", "sp", None),
            P(None, "tp", "sp"),
            P(None, "tp"),
            P(None, "tp", None),
        ),
        check_vma=False,
    )
```

profile of v0, /device:TPU:6, one launch (start us, length us, event | category | flops | bytes accessed | tf_op | source)
XLA Modules:
  0.0 266.1 jit_solution(6165527439703271470)
XLA Ops:
  7.2 1.6 pad_maximum_fusion
  8.9 1.2 dynamic-slice.3
  10.1 1.2 dynamic-slice.2
  11.4 1.7 fusion.56
  13.1 0.9 fusion.55
  14.1 1.4 fusion.34
  15.7 0.6 reduce-window.6
  16.3 0.2 slice_reduce_fusion
  16.5 0.2 reduce-window.9
  16.9 1.3 dynamic-slice
  18.8 0.2 dynamic-update-slice
  19.0 0.2 fusion.52
  19.2 0.2 dynamic-update-slice.1
  19.5 150.4 %all-reduce.3 = (f32[128]{0:T(128)S(1)}, f32[128]{0:T(128)S(1)}) all-reduce(f32[128]{0:T(128)S(1)} %dynamic-update-slice.1, f32[128]{0:T(128)S(1)} %dynamic-update-slice), channel_id=3, replica_groups=mesh['sp'=64,'tp'=8] {'sp'}, use_global_device_ids=true, to_apply=%add.2 | all-reduce | flops 256 | bytes 2048
  169.9 0.1 reshape.380
  170.1 0.5 copy.43
  170.6 0.3 reshape.398
  170.8 0.5 copy.42
  171.4 0.3 fusion.49
  171.7 0.5 fusion.43
  172.3 3.7 %fusion.16 = f32[384,256]{0,1:T(8,128)} fusion(bf16[384,4096]{1,0:T(8,128)(2,1)S(1)} %bitcast.107, bf16[4096,768]{1,0:T(8,128)(2,1)} %all-gather.4.cloned.1.call-done), kind=kOutput, calls=%fused_computation.11 | convolution fusion | flops 805502976 | bytes 5636096 | tf_op jit(solution)/shard_map/dot_general | solution.py:71
  176.0 1.2 copy.45
  177.2 0.2 fusion.19
  177.4 0.6 fusion.38
  178.0 0.1 convert_reduce_fusion
  178.1 0.7 reduce_sum.85
  178.8 0.9 multiply_bitcast_fusion
  179.7 0.7 copy.48
  180.4 6.9 %all-to-all-start.1 = ((f32[64,2,1,4]{3,1,2,0:T(2,128)}), f32[64,2,1,4]{3,1,2,0:T(2,128)}, u32[]{:S(2)}, u32[]{:S(2)}) async-start(f32[64,2,1,4]{3,1,2,0:T(2,128)} %copy.48), calls=%async_computation.1 | async-start | bytes 131072 | tf_op jit(solution)/shard_map/all_to_all | solution.py:30
  187.4 1.4 fusion.24
  188.7 4.0 %fusion.6 = bf16[512,384]{0,1:T(8,128)(2,1)S(1)} fusion(bf16[384,4096]{1,0:T(8,128)(2,1)S(1)} %bitcast.106, bf16[4096,768]{1,0:T(8,128)(2,1)} %all-gather.4.cloned.1.call-done), kind=kOutput, calls=%fused_computation.7 | convolution fusion | flops 1610809344 | bytes 7733248 | tf_op jit(solution)/shard_map/dot_general | solution.py:74
  192.8 0.2 fusion.28
  192.9 0.6 copy-done.1
  193.5 0.1 fusion.30
  193.7 8.6 %all-to-all-done.1 = f32[64,2,1,4]{3,1,2,0:T(2,128)} async-done(((f32[64,2,1,4]{3,1,2,0:T(2,128)}), f32[64,2,1,4]{3,1,2,0:T(2,128)}, u32[]{:S(2)}, u32[]{:S(2)}) %all-to-all-start.1) | async-done | bytes 2080 | tf_op jit(solution)/shard_map/all_to_all | solution.py:30
  202.4 0.9 broadcast_in_dim.22
  203.2 6.6 %all-to-all-start.2 = ((f32[64,1,1026]{2,1,0:T(1,128)}), f32[64,1,1026]{2,1,0:T(1,128)}, u32[]{:S(2)}, u32[]{:S(2)}) async-start(f32[64,1,1026]{2,1,0:T(1,128)} %broadcast_in_dim.22), calls=%async_computation.2 | async-start | bytes 589824 | tf_op jit(solution)/shard_map/all_to_all | solution.py:36
  209.9 2.3 fusion.9
  212.2 2.0 reshape.374
  214.1 2.0 copy.46
  216.2 12.9 %all-to-all-done.2 = f32[64,1,1026]{2,1,0:T(1,128)} async-done(((f32[64,1,1026]{2,1,0:T(1,128)}), f32[64,1,1026]{2,1,0:T(1,128)}, u32[]{:S(2)}, u32[]{:S(2)}) %all-to-all-start.2) | async-done | bytes 262688 | tf_op jit(solution)/shard_map/all_to_all | solution.py:36
  229.1 5.5 %all-to-all-start = ((bf16[64,4,2,1,512]{4,1,2,3,0:T(4,128)(2,1)}), bf16[64,4,2,1,512]{4,1,2,3,0:T(4,128)(2,1)}, u32[]{:S(2)}, u32[]{:S(2)}) async-start(bf16[64,4,2,1,512]{4,1,2,3,0:T(4,128)(2,1)} %copy.46), calls=%async_computation | async-start | bytes 1048576 | tf_op jit(solution)/shard_map/all_to_all | solution.py:24
  234.6 1.5 reduce_sum.86
  236.0 1.2 reduce_sum.90
  237.2 0.7 abs_maximum_fusion
  237.9 1.3 fusion.22
  239.3 18.1 %all-to-all-done = bf16[64,4,2,1,512]{4,1,2,3,0:T(4,128)(2,1)} async-done(((bf16[64,4,2,1,512]{4,1,2,3,0:T(4,128)(2,1)}), bf16[64,4,2,1,512]{4,1,2,3,0:T(4,128)(2,1)}, u32[]{:S(2)}, u32[]{:S(2)}) %all-to-all-start) | async-done | bytes 524320 | tf_op jit(solution)/shard_map/all_to_all | solution.py:24
  257.4 1.9 reduce_sum.83
  (38 shorter events, 0.9 us)
Async XLA Ops:
  7.2 4.2 %copy-start = (bf16[2,192,4096]{2,1,0:T(8,128)(2,1)S(1)}, bf16[2,192,4096]{2,1,0:T(8,128)(2,1)}, u32[]{:S(2)}) copy-start(bf16[2,192,4096]{2,1,0:T(8,128)(2,1)} %param.11) | copy-start | bytes 9437188
  7.2 5.9 %copy-start.2 = (bf16[4096,8]{0,1:T(8,128)(2,1)S(1)}, bf16[4096,8]{0,1:T(8,128)(2,1)}, u32[]{:S(2)}) copy-start(bf16[4096,8]{0,1:T(8,128)(2,1)} %param.15) | copy-start | bytes 196612
  7.2 165.1 %all-gather.4.cloned.1.call-start = ((), (), s32[]{:S(2)}) async-start(), calls=%async_computation.3 | async-start | bytes 6389760 | tf_op jit(solution)/shard_map/all_gather | solution.py:13
  13.1 158.5 %copy-start.6 = (f32[2,2,1]{1,2,0:T(1,128)S(1)}, f32[2,2,1]{1,2,0:T(1,128)}, u32[]{:S(2)}) copy-start(f32[2,2,1]{1,2,0:T(1,128)} %param.21) | copy-start | bytes 52
  171.7 4.3 %copy-start.5 = (f32[2]{0:T(128)}, f32[2]{0:T(128)S(1)}, u32[]{:S(2)}) copy-start(f32[2]{0:T(128)S(1)} %get-tuple-element.24) | copy-start | bytes 28
  172.3 4.9 %copy-start.4 = (bf16[2,1,256]{2,0,1:T(2,128)(2,1)S(1)}, bf16[2,1,256]{2,0,1:T(2,128)(2,1)}, u32[]{:S(2)}) copy-start(bf16[2,1,256]{2,0,1:T(2,128)(2,1)} %param.18) | copy-start | bytes 3076
  180.4 21.9 %all-to-all-start.1 = ((f32[64,2,1,4]{3,1,2,0:T(2,128)}), f32[64,2,1,4]{3,1,2,0:T(2,128)}, u32[]{:S(2)}, u32[]{:S(2)}) async-start(f32[64,2,1,4]{3,1,2,0:T(2,128)} %copy.48), calls=%async_computation.1 | async-start | bytes 131072 | tf_op jit(solution)/shard_map/all_to_all | solution.py:30
  188.7 4.0 %copy-start.3 = (bf16[2,192,1]{1,0,2:T(2,128)(2,1)S(1)}, bf16[2,192,1]{1,0,2:T(2,128)(2,1)}, u32[]{:S(2)}) copy-start(bf16[2,192,1]{1,0,2:T(2,128)(2,1)} %fusion.38) | copy-start | bytes 2308
  192.7 0.8 copy-start.1
  203.2 25.8 %all-to-all-start.2 = ((f32[64,1,1026]{2,1,0:T(1,128)}), f32[64,1,1026]{2,1,0:T(1,128)}, u32[]{:S(2)}, u32[]{:S(2)}) async-start(f32[64,1,1026]{2,1,0:T(1,128)} %broadcast_in_dim.22), calls=%async_computation.2 | async-start | bytes 589824 | tf_op jit(solution)/shard_map/all_to_all | solution.py:36
  229.1 28.3 %all-to-all-start = ((bf16[64,4,2,1,512]{4,1,2,3,0:T(4,128)(2,1)}), bf16[64,4,2,1,512]{4,1,2,3,0:T(4,128)(2,1)}, u32[]{:S(2)}, u32[]{:S(2)}) async-start(bf16[64,4,2,1,512]{4,1,2,3,0:T(4,128)(2,1)} %copy.46), calls=%async_computation | async-start | bytes 1048576 | tf_op jit(solution)/shard_map/all_to_all | solution.py:24
Sparse Core Ops, SparseCore 0:
  10.9 155.4 all-gather.3
where the time goes:
time: 267 us; the launch traced here: 266 us
  blocking collectives  150 us (56%)
  waiting for transfers between devices  39.7 us (15%)
  starting transfers between devices  19.1 us (7%)
  between operations  14.8 us (6%)
  other arithmetic  14.7 us (6%)
  local copies, waits for them, and re-layouts  14.2 us (5%)
  matrix products  13.1 us (5%)
    unnamed x1, blocking collectives  150 us
    all_to_all x1, waiting for transfers between devices, summed_on_arrival(): lax.all_to_all(blocks, axis, split_axis=0, concat_axis=0, tiled=True)  18.1 us
    all_to_all x1, waiting for transfers between devices, copy_for_each(): return lax.all_to_all(copies, axis, split_axis=0, concat_axis=0, tiled=True)  12.9 us
    all_to_all x1, waiting for transfers between devices, summed_on_arrival_2(): lax.all_to_all(in_blocks(value, dim, devices), axis, 0, 0, tiled=True)  8.63 us
    all_to_all x1, starting transfers between devices, summed_on_arrival_2(): lax.all_to_all(in_blocks(value, dim, devices), axis, 0, 0, tiled=True)  6.94 us
    all_to_all x1, starting transfers between devices, copy_for_each(): return lax.all_to_all(copies, axis, split_axis=0, concat_axis=0, tiled=True)  6.63 us
    all_to_all x1, starting transfers between devices, summed_on_arrival(): lax.all_to_all(blocks, axis, split_axis=0, concat_axis=0, tiled=True)  5.49 us
  transfers between devices with their start and end apart: 4, of which 3 were waited for; matrix products, arithmetic and copies ran while one was open for 11% of the time, Pallas kernels for 0%

commit v1 on v0

v1 whole, which is shorter than its diff:
```python
import jax
import jax.numpy as jnp
from jax import lax
from jax.experimental import pallas as pl
from jax.experimental.pallas import tpu as pltpu
from jax.sharding import PartitionSpec as P

F32 = jnp.float32
BF16 = jnp.bfloat16
Y = 4
KR = 256


def log_sigmoid(x):
    e = jnp.exp(-jnp.abs(x))
    series = e * (1.0 - e * (0.5 - e * (1.0 / 3.0 - e * (0.25 - e * 0.2))))
    return jnp.minimum(x, 0.0) - jnp.where(e < 0.04, series, jnp.log(1.0 + e))


def three(x):
    hi = x.astype(BF16).astype(F32)
    mid = (x - hi).astype(BF16).astype(F32)
    return hi, mid, x - hi - mid


def kernel(
    nz, nx,
    prompt, wk, wv, wi, wf, ib, fb, nq, nk, nv, ng,
    o_mem, o_norm, o_max, o_read,
    XB, WI, WF, WK, WV, AK, AV, GM, ST, PB, KC, VE, SC, SF, SB, R1, S2, R2, QM, QR, MB, RB,
    s_loc, s_ag, r_ag, s_yk, r_yk, s_sw, r_sw, s_tx, r_tx, s_st, r_st, s_qm, r_qm, s_ys, r_ys, s_zs, r_zs,
):
    sp = lax.axis_index("sp")
    tp = lax.axis_index("tp")
    z, y = sp // Y, sp % Y
    x, c = tp // 2, tp % 2
    parity = y // 2
    swapped = c != parity
    native = c == parity
    role = jnp.where(swapped, 1, 0)
    yr = jnp.where(swapped, 3 - y, y)
    yo = yr + 1 - 2 * (yr % 2)
    y1 = y + 1 - 2 * (y % 2)
    scale = 256 ** -0.5

    def at(x_, y_, z_, c_):
        return (z_ * Y + y_, x_ * 2 + c_)

    def wrap(v, n):
        return (v + n) % n

    zp, zm = at(x, y, wrap(z + 1, nz), c), at(x, y, wrap(z - 1, nz), c)
    xp, xm = at(wrap(x + 1, nx), y, z, c), at(wrap(x - 1, nx), y, z, c)
    sib, yp, diag = at(x, y, z, 1 - c), at(x, y1, z, c), at(x, y1, z, 1 - c)
    partner = at(x, 3 - y, z, 1 - c)

    def rc(src, dst, ss, rs, dev):
        return pltpu.make_async_remote_copy(
            src_ref=src, dst_ref=dst, send_sem=ss, recv_sem=rs, device_id=dev,
            device_id_type=pl.DeviceIdType.MESH)

    def rows(ref, start, n):
        return ref.at[pl.ds(pl.multiple_of(start, 32), n)]

    l_prompt = pltpu.make_async_copy(prompt, XB.at[0], s_loc.at[0])
    l_wi = pltpu.make_async_copy(wi, WI, s_loc.at[1])
    l_wf = pltpu.make_async_copy(wf, WF, s_loc.at[2])
    own_k = rows(WK, z * KR + yr * 64, 64)
    own_v = rows(WV, z * KR + yr * 64, 64)
    l_wk = pltpu.make_async_copy(wk, own_k, s_loc.at[3])
    l_wv = pltpu.make_async_copy(wv, own_v, s_loc.at[4])

    @pl.when(native)
    def _():
        l_wv.start()
        l_wk.start()

    l_prompt.start()
    l_wi.start()
    l_wf.start()

    barrier = pltpu.get_barrier_semaphore()
    for dev in (zp, zm, xp, xm, sib, yp, diag, partner):
        pl.semaphore_signal(barrier, inc=1, device_id=dev, device_id_type=pl.DeviceIdType.MESH)
    pl.semaphore_wait(barrier, 8)

    sw_v = rc(wv, rows(WV, z * KR + y * 64, 64), s_sw.at[0], r_sw.at[0], partner)
    sw_k = rc(wk, rows(WK, z * KR + y * 64, 64), s_sw.at[1], r_sw.at[1], partner)
    sw_g = rc(GM.at[0], GM.at[1], s_sw.at[2], r_sw.at[2], partner)

    def tok(xx, j, half=None):
        cols = pl.ds(pl.multiple_of((xx * 4 + j) * 256, 256), 256)
        if half is None:
            return XB.at[1, :, :, cols]
        return XB.at[1, half, :, cols]

    def sw_t(j):
        cols = pl.ds(pl.multiple_of((x * 4 + j) * 256, 256), 256)
        return rc(prompt.at[:, :, cols], tok(x, j), s_sw.at[3 + j], r_sw.at[3 + j], partner)

    def t1(way, j, xx):
        return rc(tok(xx, j), tok(xx, j), s_tx.at[way, j], r_tx.at[way, j], (xp, xm)[way])

    def t2(way, j, xx):
        q = wrap(xx - 1, nx) if way == 0 else wrap(xx + 1, nx)
        return rc(tok(q, j, way), tok(q, j, way), s_tx.at[2 + way, j], r_tx.at[2 + way, j], (xp, xm)[way])

    @pl.when(swapped)
    def _():
        sw_v.start()
        sw_k.start()
        for j in range(4):
            sw_t(j).start()

    def zk(way, s, zz):
        b = wrap(zz - (s - 1), nz) if way == 0 else wrap(zz + (s - 1), nz)
        ref = rows(WK, b * KR + c * 128, 128) if s < 8 else rows(WK, b * KR + c * 128 + way * 64, 64)
        return rc(ref, ref, s_ag.at[way, s], r_ag.at[way, s], (zp, zm)[way])

    def zv(way, s, zz, who):
        b = wrap(zz - (s - 1), nz) if way == 0 else wrap(zz + (s - 1), nz)
        ref = rows(WV, b * KR + who * 64, 64) if s < 8 else rows(WV, b * KR + who * 64 + way * 32, 32)
        return rc(ref, ref, s_ag.at[2 + way, s], r_ag.at[2 + way, s], (zp, zm)[way])

    def blocks(s):
        if s == 0 or s == 8:
            return ((0, wrap(z - s, nz)),)
        return ((0, wrap(z - s, nz)), (1, wrap(z + s, nz)))

    def yv(s, who):
        out = []
        for k, b in blocks(s):
            ref = rows(WV, b * KR + who * 64, 64)
            out.append(rc(ref, ref, s_ag.at[4 + k, s], r_ag.at[4 + k, s], yp))
        return out

    def dk(s, cc):
        out = []
        for k, b in blocks(s):
            ref = rows(WK, b * KR + cc * 128, 128)
            out.append(rc(ref, ref, s_ag.at[6 + k, s], r_ag.at[6 + k, s], sib))
        return out

    def dv(s, cc):
        out = []
        for k, b in blocks(s):
            ref = rows(WV, b * KR + cc * 128, 128)
            out.append(rc(ref, ref, s_ag.at[8 + k, s], r_ag.at[8 + k, s], sib))
        return out

    def start(copies):
        for cp in copies:
            cp.start()

    def wait_recv(copies):
        for cp in copies:
            cp.wait_recv()

    yk_send = rc(own_k, own_k, s_yk.at[0], r_yk.at[0], yp)
    other_k = rows(WK, z * KR + yo * 64, 64)
    yk_recv = rc(other_k, other_k, s_yk.at[0], r_yk.at[0], yp)
    got_v = rc(own_v, own_v, s_sw.at[0], r_sw.at[0], partner)
    got_k = rc(own_k, own_k, s_sw.at[1], r_sw.at[1], partner)

    @pl.when(native)
    def _():
        l_wv.wait()

    @pl.when(swapped)
    def _():
        got_v.wait_recv()

    zv(0, 1, z, yr).start()
    zv(1, 1, z, yr).start()

    @pl.when(native)
    def _():
        l_wk.wait()

    @pl.when(swapped)
    def _():
        got_k.wait_recv()

    yk_send.start()
    start(yv(0, yr))
    yk_recv.wait_recv()
    zk(0, 1, z).start()
    zk(1, 1, z).start()
    start(dk(0, c))

    l_prompt.wait()
    l_wi.wait()
    l_wf.wait()
    tokens = XB[0].reshape(384, 4096)
    lane8 = lax.broadcasted_iota(jnp.int32, (384, 8), 1)

    def gate(w, b):
        g = jnp.dot(tokens, w[...], preferred_element_type=F32)
        g = jnp.sum(jnp.where(lane8 == tp, g, 0.0), axis=1, keepdims=True) + b
        return jnp.broadcast_to(g, (384, 128))

    gi = gate(WI, ib[tp])
    lf = log_sigmoid(gate(WF, fb[tp]))
    after = (lax.broadcasted_iota(jnp.int32, (192, 192), 1)
             > lax.broadcasted_iota(jnp.int32, (192, 192), 0)).astype(F32)
    row8 = lax.broadcasted_iota(jnp.int32, (8, 128), 0)
    stats = jnp.zeros((8, 128), F32)
    qtile = jnp.zeros((8, 128), F32)
    for s in range(2):
        part = lf[s * 192:(s + 1) * 192]
        lw = jnp.dot(after, part, precision=lax.Precision.HIGHEST, preferred_element_type=F32)
        lw = lw + gi[s * 192:(s + 1) * 192]
        total = jnp.sum(part, axis=0, keepdims=True)
        top = jnp.max(lw, axis=0, keepdims=True)
        GM[0, s * 192:(s + 1) * 192, :] = jnp.exp(lw - top) * scale
        stats = jnp.where(row8 == 2 * s, total, jnp.where(row8 == 2 * s + 1, top, stats))
        qs = nq[s].astype(F32)
        qtile = jnp.where(row8 == 2 * s, qs[:, :128], jnp.where(row8 == 2 * s + 1, qs[:, 128:], qtile))
    GM[0, 384:392, :] = stats
    GM[0, 392:400, :] = qtile

    @pl.when(swapped)
    def _():
        sw_g.start()

    AK[...] = jnp.zeros_like(AK)
    AV[...] = jnp.zeros_like(AV)
    VE[:, 512:640] = jnp.ones((384, 128), BF16)
    kk = lax.broadcasted_iota(jnp.int32, (256, 512), 0)
    rr = lax.broadcasted_iota(jnp.int32, (256, 512), 1)
    for s in range(2):
        target = ((kk >> 2) & 3) * 128 + (kk >> 4) * 8 + s * 4 + (kk & 3)
        PB[s] = (rr == target).astype(F32).astype(BF16)

    def st(k):
        return rc(GM.at[role, pl.ds(384, 8)], ST.at[yr], s_st.at[k], r_st.at[k], (sib, yp, diag)[k])

    def step(s):
        zk(0, s, z - 1).wait_recv()
        if s < 8:
            zk(0, s + 1, z).start()
        zk(1, s, z + 1).wait_recv()
        if s < 8:
            zk(1, s + 1, z).start()
        start(dk(s, c))
        zv(0, s, z - 1, yr).wait_recv()
        if s < 8:
            zv(0, s + 1, z, yr).start()
        zv(1, s, z + 1, yr).wait_recv()
        if s < 8:
            zv(1, s + 1, z, yr).start()
        start(yv(s, yr))
        wait_recv(yv(s - 1, yo))
        start(dv(s - 1, c))

    def token_step(s):
        if s <= 5:
            @pl.when(swapped)
            def _():
                if s <= 4:
                    j = s - 1
                    got = rc(tok(x, j), tok(x, j), s_sw.at[3 + j], r_sw.at[3 + j], partner)
                    got.wait_recv()
                    t1(0, j, x).start()
                    t1(1, j, x).start()
                if s >= 2:
                    j = s - 2
                    t1(0, j, wrap(x - 1, nx)).wait_recv()
                    t2(0, j, x).start()
                    t1(1, j, wrap(x + 1, nx)).wait_recv()
                    t2(1, j, x).start()

    for s in range(1, 4):
        step(s)
        token_step(s)

    @pl.when(swapped)
    def _():
        sw_g.wait_recv()

    ST[yr] = GM[role, 384:392, :]
    for k in range(3):
        st(k).start()
    step(4)
    token_step(4)
    step(5)
    token_step(5)
    for k in range(3):
        st(k).wait_recv()
    mz, tz = [], []
    for s in range(2):
        later = jnp.zeros((1, 128), F32)
        lifts = [None] * Y
        for k in reversed(range(Y)):
            lifts[k] = ST[k, 2 * s + 1:2 * s + 2, :] + later
            later = later + ST[k, 2 * s:2 * s + 1, :]
        top = jnp.maximum(jnp.maximum(lifts[0], lifts[1]), jnp.maximum(lifts[2], lifts[3]))
        mine = lifts[3]
        for k in range(3):
            mine = jnp.where(yr == k, lifts[k], mine)
        SC[s * 192:(s + 1) * 192, :] = GM[role, s * 192:(s + 1) * 192, :] * jnp.exp(mine - top)
        mz.append(top)
        tz.append(later)
    step(6)
    step(7)

    @pl.when(swapped)
    def _():
        for j in range(4):
            t2(0, j, wrap(x - 1, nx)).wait_recv()
            t2(1, j, wrap(x + 1, nx)).wait_recv()

    def mm(b):
        xc = XB[role, :, :, pl.ds(pl.multiple_of(b * KR, KR), KR)].reshape(384, KR)
        r = pl.ds(pl.multiple_of(b * KR, KR), KR)
        AK[...] += jnp.dot(xc, WK[r, :], preferred_element_type=F32)
        AV[...] += jnp.dot(xc, WV[r, :], preferred_element_type=F32)

    def wait_d(s):
        wait_recv(dk(s, 1 - c))
        wait_recv(dv(s, 1 - c))

    def mm_pair(s):
        def one(i, carry):
            mm(wrap(z + (2 * i - 1) * s, nz))
            return carry
        lax.fori_loop(0, 2, one, 0)

    for s in range(6):
        wait_d(s)

    def early(i, carry):
        mm(wrap(z + i - 5, nz))
        return carry

    lax.fori_loop(0, 11, early, 0)
    step(8)
    wait_d(6)
    mm_pair(6)
    wait_recv(yv(8, yo))
    start(dv(8, c))
    wait_d(7)
    mm_pair(7)
    wait_d(8)
    mm(wrap(z + 8, nz))

    for s in range(2):
        sc = SC[s * 192:(s + 1) * 192, :]
        kd = (AK[s * 192:(s + 1) * 192, :] * jnp.concatenate([sc, sc], axis=1)).astype(BF16)
        KC[s * 192:(s + 1) * 192, :] = jnp.dot(kd, PB[s], preferred_element_type=F32).astype(BF16)
    VE[:, 0:512] = AV[...].astype(BF16)

    def state(h):
        cols = pl.ds(pl.multiple_of(h * 256, 256), 256)
        out = lax.dot_general(KC[:, cols], VE[...], (((0,), (0,)), ((), ())), preferred_element_type=F32)
        SF[cols, :] = out
        SB[cols, :] = out.astype(BF16)

    ys1 = rc(rows(SB, (1 - c) * 256, 256), R1, s_ys.at[0], r_ys.at[0], sib)
    ys2 = rc(S2, R2, s_ys.at[1], r_ys.at[1], yp)
    state(1 - c)
    ys1.start()
    state(c)
    qsum = []
    sf_lo = (SF[...] - SB[...].astype(F32)).astype(BF16)
    for s in range(2):
        qs = jnp.concatenate([GM[role, 392 + 2 * s:393 + 2 * s, :], GM[role, 393 + 2 * s:394 + 2 * s, :]], axis=1)
        qs = jnp.broadcast_to(qs, (16, 256)).astype(BF16)
        qc = jnp.dot(qs, PB[s], preferred_element_type=F32).astype(BF16)
        full = jnp.dot(qc, SB[...], preferred_element_type=F32) + jnp.dot(qc, sf_lo, preferred_element_type=F32)
        qsum.append(full[0:8])
    row640 = lax.broadcasted_iota(jnp.int32, (8, 640), 0)
    both = jnp.where(row640 < 4, qsum[0], qsum[1])
    qt = jnp.zeros((8, 128), F32)
    for k in range(4):
        qt = qt + jnp.where((row8 & 3) == k, both[:, k * 128:(k + 1) * 128], 0.0)
    QM[0:8, :] = qt
    QM[8:16, :] = both[:, 512:640]

    def qm(k):
        return rc(QM, QR.at[k], s_qm.at[k], r_qm.at[k], (sib, yp, diag)[k])

    for k in range(3):
        qm(k).start()
    ys1.wait_recv()
    send_rows = pl.ds(pl.multiple_of(yo * 128, 128), 128)
    keep_rows = pl.ds(pl.multiple_of(yr * 128, 128), 128)
    send_part = pl.ds(pl.multiple_of((yo % 2) * 128, 128), 128)
    keep_part = pl.ds(pl.multiple_of((yr % 2) * 128, 128), 128)
    S2[...] = (SF[send_rows, :] + R1[send_part, :].astype(F32)).astype(BF16)
    ys2.start()
    kept = SF[keep_rows, :] + R1[keep_part, :].astype(F32)
    for k in range(3):
        qm(k).wait_recv()
    qall = QM[...] + QR[0] + QR[1] + QR[2]
    qt, qn = qall[0:8], qall[8:16]
    lane8 = lax.broadcasted_iota(jnp.int32, (8, 128), 1)
    head = jnp.zeros((8, 128), F32)
    m8 = jnp.where(row8 < 4, mz[0], mz[1])
    t8 = jnp.where(row8 < 4, tz[0], tz[1])
    for base, v in ((2, m8), (5, t8), (8, qn)):
        for i, piece in enumerate(three(v)):
            head = jnp.where(lane8 == base + i, piece, head)
    MB[:, :, 640:768] = jnp.broadcast_to(qt.astype(BF16)[None], (nz, 8, 128))
    ys2.wait_recv()
    kept = (kept + R2[...].astype(F32)).reshape(nz, 8, 640)
    MB[:, :, 0:512] = kept[:, :, 0:512].astype(BF16)
    norm = kept[:, :, 512:640]
    norm_hi = norm.astype(BF16).astype(F32)
    lane3 = lax.broadcasted_iota(jnp.int32, (nz, 8, 128), 2)
    tail = jnp.where(lane3 == 0, norm_hi, jnp.where(lane3 == 1, norm - norm_hi, head[None]))
    MB[:, :, 512:640] = tail.astype(BF16)

    oy = jnp.where(swapped, 3 - y, y)
    oc = jnp.where(swapped, 1 - c, c)

    def zs(to):
        return rc(MB.at[to], RB.at[z], s_zs.at[to], r_zs.at[z], at(x, oy, to, oc))

    def zs_recv(frm):
        return rc(MB.at[frm], RB.at[frm], s_zs.at[frm], r_zs.at[frm], at(x, oy, frm, oc))

    for d in (8, 7, -7, 6, -6, 5, -5, 4, -4, 3, -3, 2, -2, 1, -1):
        zs(wrap(z + d, nz)).start()

    @pl.when(swapped)
    def _():
        zs(z).start()

    @pl.when(native)
    def _():
        RB[z] = MB[z]

    for d in (1, -1, 2, -2, 3, -3, 4, -4, 5, -5, 6, -6, 7, -7, 8):
        zs_recv(wrap(z + d, nz)).wait_recv()

    @pl.when(swapped)
    def _():
        zs_recv(z).wait_recv()

    tails = RB[:, :, 512:640].astype(F32)
    m_all = jnp.sum(jnp.where((lane3 >= 2) & (lane3 < 5), tails, 0.0), axis=2, keepdims=True)
    t_all = jnp.sum(jnp.where((lane3 >= 5) & (lane3 < 8), tails, 0.0), axis=2, keepdims=True)
    later = jnp.zeros((8, 1), F32)
    lifts = [None] * nz
    for k in reversed(range(nz)):
        lifts[k] = m_all[k] + later
        later = later + t_all[k]
    top = lifts[0]
    for k in range(1, nz):
        top = jnp.maximum(top, lifts[k])
    acc = jnp.zeros((8, 768), F32)
    for k in range(nz):
        acc = acc + jnp.exp(lifts[k] - top) * RB[k].astype(F32)
    for s in range(2):
        o_mem[s, 0] = acc[4 * s:4 * s + 4, 0:512].astype(BF16)
        o_max[s] = top[4 * s]
    tail = acc[:, 512:640]
    norm = jnp.sum(jnp.where(lane8 < 2, tail, 0.0), axis=1, keepdims=True)
    qn = jnp.sum(jnp.where((lane8 >= 8) & (lane8 < 11), tail, 0.0), axis=1, keepdims=True)
    for s in range(2):
        line = jnp.sum(jnp.where(row8 - 4 * s == lane8, norm, 0.0), axis=0, keepdims=True)
        o_norm[s] = line[:, 0:4]
    row1 = lax.broadcasted_iota(jnp.int32, (8, 1), 0)
    gate_in = jnp.where(row1 < 4, ng[0, 0:1, :], ng[0, 1:2, :])
    gate_forget = log_sigmoid(jnp.where(row1 < 4, ng[1, 0:1, :], ng[1, 1:2, :]))
    own = [jnp.sum(nq[s].astype(F32) * nk[s].astype(F32), axis=1, keepdims=True) * scale for s in range(2)]
    own = jnp.where(row1 < 4, own[0], own[1])
    mixed = jnp.maximum(gate_forget + top, gate_in)
    carried = jnp.exp(gate_forget + top - mixed)
    fresh = jnp.exp(gate_in - mixed)
    value = jnp.zeros((8, 128), F32)
    for s in range(2):
        for k in range(4):
            value = jnp.where(row8 == 4 * s + k, nv[s].astype(F32)[:, k * 128:(k + 1) * 128], value)
    numer = carried * acc[:, 640:768] + fresh * own * value
    denom = carried * qn + fresh * own
    read = numer / jnp.maximum(jnp.abs(denom), 1.0)
    for s in range(2):
        for k in range(4):
            o_read[s, :, k * 128:(k + 1) * 128] = read[4 * s + k:4 * s + k + 1].astype(BF16)

    for s in range(1, 9):
        for way in range(2):
            zk(way, s, z).wait_send()
            zv(way, s, z, yr).wait_send()
    for s in range(9):
        for cp in yv(s, yr) + dk(s, c) + dv(s, c):
            cp.wait_send()
    yk_send.wait_send()
    for k in range(3):
        st(k).wait_send()
        qm(k).wait_send()
    ys1.wait_send()
    ys2.wait_send()
    for d in range(1, 16):
        zs(wrap(z + d - 16, nz)).wait_send()

    @pl.when(swapped)
    def _():
        zs(z).wait_send()
        sw_v.wait_send()
        sw_k.wait_send()
        sw_g.wait_send()
        for j in range(4):
            sw_t(j).wait_send()
            for way in range(2):
                t1(way, j, x).wait_send()
                t2(way, j, x).wait_send()


def per_device(*args):
    nz = lax.axis_size("sp") // Y
    nx = lax.axis_size("tp") // 2
    vm = pl.BlockSpec(memory_space=pltpu.VMEM)
    sm = pl.BlockSpec(memory_space=pltpu.SMEM)
    hb = pl.BlockSpec(memory_space=pltpu.HBM)
    dma = pltpu.SemaphoreType.DMA
    return pl.pallas_call(
        lambda *refs: kernel(nz, nx, *refs),
        out_shape=(
            jax.ShapeDtypeStruct((2, 1, 4, 512), BF16),
            jax.ShapeDtypeStruct((2, 1, 4), F32),
            jax.ShapeDtypeStruct((2, 1), F32),
            jax.ShapeDtypeStruct((2, 1, 512), BF16),
        ),
        in_specs=[hb] * 5 + [sm] * 2 + [vm] * 4,
        out_specs=(vm,) * 4,
        scratch_shapes=[
            pltpu.VMEM((2, 2, 192, 4096), BF16),
            pltpu.VMEM((4096, 8), BF16),
            pltpu.VMEM((4096, 8), BF16),
            pltpu.VMEM((4096, 256), BF16),
            pltpu.VMEM((4096, 512), BF16),
            pltpu.VMEM((384, 256), F32),
            pltpu.VMEM((384, 512), F32),
            pltpu.VMEM((2, 400, 128), F32),
            pltpu.VMEM((4, 8, 128), F32),
            pltpu.VMEM((2, 256, 512), BF16),
            pltpu.VMEM((384, 512), BF16),
            pltpu.VMEM((384, 640), BF16),
            pltpu.VMEM((384, 128), F32),
            pltpu.VMEM((512, 640), F32),
            pltpu.VMEM((512, 640), BF16),
            pltpu.VMEM((256, 640), BF16),
            pltpu.VMEM((128, 640), BF16),
            pltpu.VMEM((128, 640), BF16),
            pltpu.VMEM((16, 128), F32),
            pltpu.VMEM((3, 16, 128), F32),
            pltpu.VMEM((nz, 8, 768), BF16),
            pltpu.VMEM((nz, 8, 768), BF16),
            dma((5,)),
            dma((10, 9)), dma((10, 9)),
            dma((1,)), dma((1,)),
            dma((7,)), dma((7,)),
            dma((4, 4)), dma((4, 4)),
            dma((3,)), dma((3,)),
            dma((3,)), dma((3,)),
            dma((2,)), dma((2,)),
            dma((nz,)), dma((nz,)),
        ],
        compiler_params=pltpu.CompilerParams(
            collective_id=0, has_side_effects=True, vmem_limit_bytes=56 * 1024 * 1024),
        name="prefill",
    )(*args)


def solution(mesh):
    placed = (
        P(None, "sp", None),
        P("sp", "tp"),
        P("sp", "tp"),
        P(),
        P(),
        P(),
        P(),
        P(None, "tp", None),
        P(None, "tp", None),
        P(None, "tp", None),
        P(None, None, "tp"),
    )
    return jax.shard_map(
        per_device,
        mesh=mesh,
        in_specs=placed,
        out_specs=(
            P(None, "tp", "sp", None),
            P(None, "tp", "sp"),
            P(None, "tp"),
            P(None, "tp", None),
        ),
        check_vma=False,
    )
```

time: 267 us -> 96.9 us (0.36)
  the two profiles are of different devices: /device:TPU:6 before, /device:TPU:1 now
where the time goes in v1:
time: 96.9 us; the launch traced here: 96.4 us
  Pallas kernels  81.2 us (84%)
  local copies, waits for them, and re-layouts  14.6 us (15%)
    pallas_call x1, Pallas kernels, per_device(): pl.pallas_call(lambda *refs: kernel(nz, nx, *refs), out_shape=(jax.ShapeD...  81.2 us
    unnamed x8, local copies, waits for them, and re-layouts  12 us
    pallas_call x2, local copies, waits for them, and re-layouts, per_device(): pl.pallas_call(lambda *refs: kernel(nz, nx, *refs), out_shape=(jax.ShapeD...  2.52 us

profile of v1, /device:TPU:1, one launch (start us, length us, event | category | flops | bytes accessed | tf_op | source)
XLA Modules:
  0.0 96.4 jit_solution(15170201090847056782)
XLA Ops:
  0.6 1.3 %copy.17.refs_7_ = bf16[2,1,256]{2,1,0:T(2,128)(2,1)} copy(bf16[2,1,256]{2,0,1:T(2,128)(2,1)} %param.18) | data formatting | bytes 2048 | tf_op args[7]
  1.9 1.3 %copy.18.refs_8_ = bf16[2,1,256]{2,1,0:T(2,128)(2,1)} copy(bf16[2,1,256]{2,0,1:T(2,128)(2,1)} %param.19) | data formatting | bytes 2048 | tf_op args[8]
  3.2 1.3 %copy.20.refs_10_ = f32[2,2,1]{2,1,0:T(2,128)} copy(f32[2,2,1]{1,2,0:T(1,128)} %param.21) | data formatting | bytes 32 | tf_op args[10]
  4.5 1.3 %copy.19.refs_9_ = bf16[2,1,512]{2,1,0:T(2,128)(2,1)} copy(bf16[2,1,512]{2,0,1:T(2,128)(2,1)} %param.20) | data formatting | bytes 4096 | tf_op args[9]
  5.8 2.2 %copy.15.refs_3_ = bf16[4096,8]{1,0:T(8,128)(2,1)} copy(bf16[4096,8]{0,1:T(8,128)(2,1)} %param.14) | data formatting | bytes 131072 | tf_op args[3]
  8.0 2.2 %copy.16.refs_4_ = bf16[4096,8]{1,0:T(8,128)(2,1)} copy(bf16[4096,8]{0,1:T(8,128)(2,1)} %param.15) | data formatting | bytes 131072 | tf_op args[4]
  10.2 81.2 %prefill.1 = (bf16[2,1,4,512]{3,2,1,0:T(4,128)(2,1)}, f32[2,1,4]{2,1,0:T(1,128)}, f32[2,1]{1,0:T(2,128)}, bf16[2,1,512]{2,1,0:T(2,128)(2,1)}) custom-call(bf16[2,192,4096]{2,1,0:T(8,128)(2,1)} %refs_0_.1, bf16[64,256]{1,0:T(8,128)(2,1)} %refs_1_.1, bf16[64,512]{1,0:T(8,128)(2,1)} %refs_2_.1, bf16[4096,8]{1,0:T(8,128)(2,1)} %copy.15.refs_3_, ...), custom_call_target="tpu_custom_call" | custom-call | tf_op jit(solution)/shard_map/prefill/pallas_call | solution.py:519
  91.4 1.3 %copy.21 = f32[2,1]{0,1:T(1,128)} copy(f32[2,1]{1,0:T(2,128)} %get-tuple-element.6) | data formatting | bytes 16 | tf_op jit(solution)/shard_map/prefill/pallas_call | solution.py:519
  92.7 1.3 %copy.22 = bf16[2,1,512]{2,0,1:T(2,128)(2,1)} copy(bf16[2,1,512]{2,1,0:T(2,128)(2,1)} %get-tuple-element.7) | data formatting | bytes 4096 | tf_op jit(solution)/shard_map/prefill/pallas_call | solution.py:519
  93.9 1.3 %copy.25 = bf16[2,1,4,512]{3,2,1,0:T(4,128)(2,1)} copy(bf16[2,1,4,512]{3,2,1,0:T(4,128)(2,1)} %get-tuple-element.12) | data formatting | bytes 16384
  95.2 1.2 %copy.26 = f32[2,1,4]{2,1,0:T(1,128)} copy(f32[2,1,4]{2,1,0:T(1,128)} %get-tuple-element.13) | data formatting | bytes 64

commit v2 on v1

--- a/solution.py
+++ b/solution.py
@@ -26,7 +26,7 @@
 def kernel(
     nz, nx,
     prompt, wk, wv, wi, wf, ib, fb, nq, nk, nv, ng,
-    o_mem, o_norm, o_max, o_read,
+    out,
     XB, WI, WF, WK, WV, AK, AV, GM, ST, PB, KC, VE, SC, SF, SB, R1, S2, R2, QM, QR, MB, RB,
     s_loc, s_ag, r_ag, s_yk, r_yk, s_sw, r_sw, s_tx, r_tx, s_st, r_st, s_qm, r_qm, s_ys, r_ys, s_zs, r_zs,
 ):
@@ -195,7 +195,7 @@
     lane8 = lax.broadcasted_iota(jnp.int32, (384, 8), 1)
 
     def gate(w, b):
-        g = jnp.dot(tokens, w[...], preferred_element_type=F32)
+        g = lax.dot_general(tokens, w[...], (((1,), (1,)), ((), ())), preferred_element_type=F32)
         g = jnp.sum(jnp.where(lane8 == tp, g, 0.0), axis=1, keepdims=True) + b
         return jnp.broadcast_to(g, (384, 128))
 
@@ -214,7 +214,7 @@
         top = jnp.max(lw, axis=0, keepdims=True)
         GM[0, s * 192:(s + 1) * 192, :] = jnp.exp(lw - top) * scale
         stats = jnp.where(row8 == 2 * s, total, jnp.where(row8 == 2 * s + 1, top, stats))
-        qs = nq[s].astype(F32)
+        qs = nq[s:s + 1, :].astype(F32)
         qtile = jnp.where(row8 == 2 * s, qs[:, :128], jnp.where(row8 == 2 * s + 1, qs[:, 128:], qtile))
     GM[0, 384:392, :] = stats
     GM[0, 392:400, :] = qtile
@@ -452,19 +452,13 @@
     acc = jnp.zeros((8, 768), F32)
     for k in range(nz):
         acc = acc + jnp.exp(lifts[k] - top) * RB[k].astype(F32)
-    for s in range(2):
-        o_mem[s, 0] = acc[4 * s:4 * s + 4, 0:512].astype(BF16)
-        o_max[s] = top[4 * s]
     tail = acc[:, 512:640]
     norm = jnp.sum(jnp.where(lane8 < 2, tail, 0.0), axis=1, keepdims=True)
     qn = jnp.sum(jnp.where((lane8 >= 8) & (lane8 < 11), tail, 0.0), axis=1, keepdims=True)
-    for s in range(2):
-        line = jnp.sum(jnp.where(row8 - 4 * s == lane8, norm, 0.0), axis=0, keepdims=True)
-        o_norm[s] = line[:, 0:4]
     row1 = lax.broadcasted_iota(jnp.int32, (8, 1), 0)
-    gate_in = jnp.where(row1 < 4, ng[0, 0:1, :], ng[0, 1:2, :])
-    gate_forget = log_sigmoid(jnp.where(row1 < 4, ng[1, 0:1, :], ng[1, 1:2, :]))
-    own = [jnp.sum(nq[s].astype(F32) * nk[s].astype(F32), axis=1, keepdims=True) * scale for s in range(2)]
+    gate_in = jnp.where(row1 < 4, ng[0, :, 0:1], ng[0, :, 1:2])
+    gate_forget = log_sigmoid(jnp.where(row1 < 4, ng[1, :, 0:1], ng[1, :, 1:2]))
+    own = [jnp.sum(nq[s:s + 1, :].astype(F32) * nk[s:s + 1, :].astype(F32), axis=1, keepdims=True) * scale for s in range(2)]
     own = jnp.where(row1 < 4, own[0], own[1])
     mixed = jnp.maximum(gate_forget + top, gate_in)
     carried = jnp.exp(gate_forget + top - mixed)
@@ -472,13 +466,13 @@
     value = jnp.zeros((8, 128), F32)
     for s in range(2):
         for k in range(4):
-            value = jnp.where(row8 == 4 * s + k, nv[s].astype(F32)[:, k * 128:(k + 1) * 128], value)
+            value = jnp.where(row8 == 4 * s + k, nv[s:s + 1, k * 128:(k + 1) * 128].astype(F32), value)
     numer = carried * acc[:, 640:768] + fresh * own * value
     denom = carried * qn + fresh * own
     read = numer / jnp.maximum(jnp.abs(denom), 1.0)
-    for s in range(2):
-        for k in range(4):
-            o_read[s, :, k * 128:(k + 1) * 128] = read[4 * s + k:4 * s + k + 1].astype(BF16)
+    out[:, 0:512] = acc[:, 0:512]
+    out[:, 512:640] = jnp.where(lane8 == 0, top, norm)
+    out[:, 640:768] = read
 
     for s in range(1, 9):
         for way in range(2):
@@ -509,27 +503,38 @@
                 t2(way, j, x).wait_send()
 
 
-def per_device(*args):
+def unpack(got, o_mem, o_norm, o_max, o_read):
+    row = lax.broadcasted_iota(jnp.int32, (8, 128), 0)
+    lane = lax.broadcasted_iota(jnp.int32, (8, 128), 1)
+    tail = got[:, 512:640]
+    top, norm = tail[:, 0:1], tail[:, 1:2]
+    o_max[...] = jnp.sum(jnp.where(row == 4 * lane, top, 0.0), axis=0, keepdims=True)[:, 0:2]
+    for s in range(2):
+        o_mem[s, 0] = got[4 * s:4 * s + 4, 0:512].astype(BF16)
+        line = jnp.sum(jnp.where(row - 4 * s == lane, norm, 0.0), axis=0, keepdims=True)
+        o_norm[s] = line[:, 0:4]
+        for k in range(4):
+            at = 4 * s + k
+            o_read[s:s + 1, k * 128:(k + 1) * 128] = got[at:at + 1, 640:768].astype(BF16)
+
+
+def per_device(prompt, w_key, w_value, w_igate, w_fgate, input_bias, forget_bias, new_query, new_key, new_value,
+               new_gates):
     nz = lax.axis_size("sp") // Y
     nx = lax.axis_size("tp") // 2
     vm = pl.BlockSpec(memory_space=pltpu.VMEM)
     sm = pl.BlockSpec(memory_space=pltpu.SMEM)
     hb = pl.BlockSpec(memory_space=pltpu.HBM)
     dma = pltpu.SemaphoreType.DMA
-    return pl.pallas_call(
+    packed = pl.pallas_call(
         lambda *refs: kernel(nz, nx, *refs),
-        out_shape=(
-            jax.ShapeDtypeStruct((2, 1, 4, 512), BF16),
-            jax.ShapeDtypeStruct((2, 1, 4), F32),
-            jax.ShapeDtypeStruct((2, 1), F32),
-            jax.ShapeDtypeStruct((2, 1, 512), BF16),
-        ),
+        out_shape=jax.ShapeDtypeStruct((8, 768), F32),
         in_specs=[hb] * 5 + [sm] * 2 + [vm] * 4,
-        out_specs=(vm,) * 4,
+        out_specs=vm,
         scratch_shapes=[
             pltpu.VMEM((2, 2, 192, 4096), BF16),
-            pltpu.VMEM((4096, 8), BF16),
-            pltpu.VMEM((4096, 8), BF16),
+            pltpu.VMEM((8, 4096), BF16),
+            pltpu.VMEM((8, 4096), BF16),
             pltpu.VMEM((4096, 256), BF16),
             pltpu.VMEM((4096, 512), BF16),
             pltpu.VMEM((384, 256), F32),
@@ -562,7 +567,24 @@
         compiler_params=pltpu.CompilerParams(
             collective_id=0, has_side_effects=True, vmem_limit_bytes=56 * 1024 * 1024),
         name="prefill",
-    )(*args)
+    )(
+        prompt, w_key, w_value, w_igate.T, w_fgate.T, input_bias, forget_bias,
+        new_query.reshape(2, 256), new_key.reshape(2, 256), new_value.reshape(2, 512),
+        jnp.transpose(new_gates, (0, 2, 1)),
+    )
+    mem, norm, top, read = pl.pallas_call(
+        unpack,
+        out_shape=(
+            jax.ShapeDtypeStruct((2, 1, 4, 512), BF16),
+            jax.ShapeDtypeStruct((2, 1, 4), F32),
+            jax.ShapeDtypeStruct((1, 2), F32),
+            jax.ShapeDtypeStruct((2, 512), BF16),
+        ),
+        in_specs=[vm],
+        out_specs=(vm,) * 4,
+        name="unpack",
+    )(packed)
+    return mem, norm, top.T, read.reshape(2, 1, 512)
 
 
 def solution(mesh):

time: 96.9 us -> 83.4 us (0.86)
  local copies, waits for them, and re-layouts: 14.6 us -> 0 us
  Pallas kernels: 81.2 us -> 82.6 us
    unnamed x8 -> x0, local copies, waits for them, and re-layouts: 12 us -> none
    pallas_call x2 -> x0, local copies, waits for them, and re-layouts: 2.52 us -> none  [per_device(): pl.pallas_call(lambda *refs: kernel(nz, nx, *refs), out_shape=(jax.ShapeD...]
    pallas_call x1 -> x2, Pallas kernels: 81.2 us -> 82.6 us  [the longest x1 81.2 us: per_device(): pl.pallas_call(lambda *refs: kernel(nz, nx, *refs), out_shape=jax.ShapeDt...]
where the time goes in v2:
time: 83.4 us; the launch traced here: 83.2 us
  Pallas kernels  82.6 us (99%)
    pallas_call x1, Pallas kernels, per_device(): pl.pallas_call(lambda *refs: kernel(nz, nx, *refs), out_shape=jax.ShapeDt...  81.2 us

profile of v2, /device:TPU:1, one launch (start us, length us, event | category | flops | bytes accessed | tf_op | source)
XLA Modules:
  0.0 83.2 jit_solution(6068705151874072234)
XLA Ops:
  0.6 81.2 %prefill.1.got = f32[8,768]{1,0:T(8,128)} custom-call(bf16[2,192,4096]{2,1,0:T(8,128)(2,1)} %refs_0_.1, bf16[64,256]{1,0:T(8,128)(2,1)} %refs_1_.1, bf16[64,512]{1,0:T(8,128)(2,1)} %refs_2_.1, bf16[8,4096]{1,0:T(8,128)(2,1)} %bitcast.10, bf16[8,4096]{1,0:T(8,128)(2,1)} %bitcast.11, f32[8]{0:T(128)} %refs_5_.1, f32[8]{0:T(128)} %refs_6_.1, ...), custom_call_target="tpu_custom_call" | custom-call | tf_op jit(solution)/shard_map/prefill/pallas_call | solution.py:529
  81.8 1.4 %unpack.1 = (bf16[2,1,4,512]{3,2,1,0:T(4,128)(2,1)}, f32[2,1,4]{2,1,0:T(1,128)}, f32[1,2]{1,0:T(1,128)}, bf16[2,512]{1,0:T(2,128)(2,1)}) custom-call(f32[8,768]{1,0:T(8,128)} %prefill.1.got), custom_call_target="tpu_custom_call" | custom-call | tf_op jit(solution)/shard_map/unpack/pallas_call | solution.py:575

commit v3 on v2

--- a/solution.py
+++ b/solution.py
@@ -8,6 +8,7 @@
 F32 = jnp.float32
 BF16 = jnp.bfloat16
 Y = 4
+GROUP = (0, 0, 0, 1, 1, 2, 2, 3, 4)
 KR = 256
 
 
@@ -25,10 +26,12 @@
 
 def kernel(
     nz, nx,
-    prompt, wk, wv, wi, wf, ib, fb, nq, nk, nv, ng,
+    prompt, wk, wv, wi, wf, h_ib, h_fb, h_nq, h_nk, h_nv, h_ng,
     out,
-    XB, WI, WF, WK, WV, AK, AV, GM, ST, PB, KC, VE, SC, SF, SB, R1, S2, R2, QM, QR, MB, RB,
-    s_loc, s_ag, r_ag, s_yk, r_yk, s_sw, r_sw, s_tx, r_tx, s_st, r_st, s_qm, r_qm, s_ys, r_ys, s_zs, r_zs,
+    XB, WI, WF, WK, WV, AK, AV, GM, ST, PB, KC, VE, SC, SF, SB, R1, S2, R2, QM, QR, MA, MB, RA, RB,
+    ib, fb, nq, nk, nv, ng,
+    s_loc, s_k, s_v, s_y, s_d, r_z, r_y, r_d, s_yk, r_yk, s_sw, r_sw, s_t, r_t1, r_t2,
+    s_st, r_st, s_qm, r_qm, s_ys, r_ys, s_zs, r_zs,
 ):
     sp = lax.axis_index("sp")
     tp = lax.axis_index("tp")
@@ -62,6 +65,10 @@
     def rows(ref, start, n):
         return ref.at[pl.ds(pl.multiple_of(start, 32), n)]
 
+    barrier = pltpu.get_barrier_semaphore()
+    for dev in (zp, zm, xp, xm, sib, yp, diag, partner):
+        pl.semaphore_signal(barrier, inc=1, device_id=dev, device_id_type=pl.DeviceIdType.MESH)
+
     l_prompt = pltpu.make_async_copy(prompt, XB.at[0], s_loc.at[0])
     l_wi = pltpu.make_async_copy(wi, WI, s_loc.at[1])
     l_wf = pltpu.make_async_copy(wf, WF, s_loc.at[2])
@@ -78,15 +85,21 @@
     l_prompt.start()
     l_wi.start()
     l_wf.start()
-
-    barrier = pltpu.get_barrier_semaphore()
-    for dev in (zp, zm, xp, xm, sib, yp, diag, partner):
-        pl.semaphore_signal(barrier, inc=1, device_id=dev, device_id_type=pl.DeviceIdType.MESH)
+    small = [pltpu.make_async_copy(a, b, s_loc.at[5 + i]) for i, (a, b) in enumerate(
+        ((h_ib, ib), (h_fb, fb), (h_nq, nq), (h_nk, nk), (h_nv, nv), (h_ng, ng)))]
+    for cp in small:
+        cp.start()
     pl.semaphore_wait(barrier, 8)
 
     sw_v = rc(wv, rows(WV, z * KR + y * 64, 64), s_sw.at[0], r_sw.at[0], partner)
-    sw_k = rc(wk, rows(WK, z * KR + y * 64, 64), s_sw.at[1], r_sw.at[1], partner)
-    sw_g = rc(GM.at[0], GM.at[1], s_sw.at[2], r_sw.at[2], partner)
+    sw_k = rc(wk, rows(WK, z * KR + y * 64, 64), s_sw.at[0], r_sw.at[1], partner)
+    sw_g = rc(GM.at[0], GM.at[1], s_sw.at[1], r_sw.at[2], partner)
+
+    def all_sent(ref, sem):
+        rc(ref, ref, sem, sem, partner).wait_send()
+
+    def all_here(ref, sem):
+        rc(ref, ref, sem, sem, partner).wait_recv()
 
     def tok(xx, j, half=None):
         cols = pl.ds(pl.multiple_of((xx * 4 + j) * 256, 256), 256)
@@ -96,14 +109,14 @@
 
     def sw_t(j):
         cols = pl.ds(pl.multiple_of((x * 4 + j) * 256, 256), 256)
-        return rc(prompt.at[:, :, cols], tok(x, j), s_sw.at[3 + j], r_sw.at[3 + j], partner)
+        return rc(prompt.at[:, :, cols], tok(x, j), s_sw.at[2], r_sw.at[3 + j], partner)
 
     def t1(way, j, xx):
-        return rc(tok(xx, j), tok(xx, j), s_tx.at[way, j], r_tx.at[way, j], (xp, xm)[way])
+        return rc(tok(xx, j), tok(xx, j), s_t.at[0], r_t1.at[way, j], (xp, xm)[way])
 
     def t2(way, j, xx):
         q = wrap(xx - 1, nx) if way == 0 else wrap(xx + 1, nx)
-        return rc(tok(q, j, way), tok(q, j, way), s_tx.at[2 + way, j], r_tx.at[2 + way, j], (xp, xm)[way])
+        return rc(tok(q, j, way), tok(q, j, way), s_t.at[1], r_t2.at[0], (xp, xm)[way])
 
     @pl.when(swapped)
     def _():
@@ -112,15 +125,17 @@
         for j in range(4):
             sw_t(j).start()
 
-    def zk(way, s, zz):
+    def zc(st, way, s, zz):
         b = wrap(zz - (s - 1), nz) if way == 0 else wrap(zz + (s - 1), nz)
-        ref = rows(WK, b * KR + c * 128, 128) if s < 8 else rows(WK, b * KR + c * 128 + way * 64, 64)
-        return rc(ref, ref, s_ag.at[way, s], r_ag.at[way, s], (zp, zm)[way])
-
-    def zv(way, s, zz, who):
-        b = wrap(zz - (s - 1), nz) if way == 0 else wrap(zz + (s - 1), nz)
-        ref = rows(WV, b * KR + who * 64, 64) if s < 8 else rows(WV, b * KR + who * 64 + way * 32, 32)
-        return rc(ref, ref, s_ag.at[2 + way, s], r_ag.at[2 + way, s], (zp, zm)[way])
+        if st < 2:
+            ref = rows(WK, b * KR + (yr, yo)[st] * 64, 64)
+        else:
+            ref = rows(WV, b * KR + yr * 64 + (st - 2) * 32, 32)
+        slot = st * 15 + (14 if s == 8 else way * 7 + s - 1)
+        return rc(ref, ref, (s_k if st < 2 else s_v).at[0], r_z.at[slot], (zp, zm)[way])
+
+    def ways(st, s):
+        return (0, 1) if s < 8 else (st % 2,)
 
     def blocks(s):
         if s == 0 or s == 8:
@@ -131,30 +146,33 @@
         out = []
         for k, b in blocks(s):
             ref = rows(WV, b * KR + who * 64, 64)
-            out.append(rc(ref, ref, s_ag.at[4 + k, s], r_ag.at[4 + k, s], yp))
+            out.append(rc(ref, ref, s_y.at[0], r_y.at[s], yp))
         return out
 
     def dk(s, cc):
         out = []
         for k, b in blocks(s):
             ref = rows(WK, b * KR + cc * 128, 128)
-            out.append(rc(ref, ref, s_ag.at[6 + k, s], r_ag.at[6 + k, s], sib))
+            out.append(rc(ref, ref, s_d.at[0], r_d.at[GROUP[s]], sib))
         return out
 
     def dv(s, cc):
         out = []
         for k, b in blocks(s):
             ref = rows(WV, b * KR + cc * 128, 128)
-            out.append(rc(ref, ref, s_ag.at[8 + k, s], r_ag.at[8 + k, s], sib))
+            out.append(rc(ref, ref, s_d.at[0], r_d.at[GROUP[s]], sib))
         return out
 
     def start(copies):
         for cp in copies:
             cp.start()
 
-    def wait_recv(copies):
-        for cp in copies:
-            cp.wait_recv()
+    def y_here(s):
+        all_here(rows(WV, 0, 64 * len(blocks(s))), r_y.at[s])
+
+    def d_here(g):
+        n = sum(len(blocks(s)) for s in range(9) if GROUP[s] == g)
+        all_here(rows(WV, 0, 192 * n), r_d.at[g])
 
     yk_send = rc(own_k, own_k, s_yk.at[0], r_yk.at[0], yp)
     other_k = rows(WK, z * KR + yo * 64, 64)
@@ -170,8 +188,10 @@
     def _():
         got_v.wait_recv()
 
-    zv(0, 1, z, yr).start()
-    zv(1, 1, z, yr).start()
+    for st in (2, 3):
+        for way in (0, 1):
+            zc(st, way, 1, z).start()
+    start(yv(0, yr))
 
     @pl.when(native)
     def _():
@@ -182,25 +202,23 @@
         got_k.wait_recv()
 
     yk_send.start()
-    start(yv(0, yr))
-    yk_recv.wait_recv()
-    zk(0, 1, z).start()
-    zk(1, 1, z).start()
-    start(dk(0, c))
-
+    for way in (0, 1):
+        zc(0, way, 1, z).start()
     l_prompt.wait()
     l_wi.wait()
     l_wf.wait()
+    for cp in small:
+        cp.wait()
     tokens = XB[0].reshape(384, 4096)
     lane8 = lax.broadcasted_iota(jnp.int32, (384, 8), 1)
 
     def gate(w, b):
         g = lax.dot_general(tokens, w[...], (((1,), (1,)), ((), ())), preferred_element_type=F32)
-        g = jnp.sum(jnp.where(lane8 == tp, g, 0.0), axis=1, keepdims=True) + b
+        g = jnp.sum(jnp.where(lane8 == tp, g + b[...], 0.0), axis=1, keepdims=True)
         return jnp.broadcast_to(g, (384, 128))
 
-    gi = gate(WI, ib[tp])
-    lf = log_sigmoid(gate(WF, fb[tp]))
+    gi = gate(WI, ib)
+    lf = log_sigmoid(gate(WF, fb))
     after = (lax.broadcasted_iota(jnp.int32, (192, 192), 1)
              > lax.broadcasted_iota(jnp.int32, (192, 192), 0)).astype(F32)
     row8 = lax.broadcasted_iota(jnp.int32, (8, 128), 0)
@@ -223,6 +241,11 @@
     def _():
         sw_g.start()
 
+    yk_recv.wait_recv()
+    for way in (0, 1):
+        zc(1, way, 1, z).start()
+    start(dk(0, c))
+
     AK[...] = jnp.zeros_like(AK)
     AV[...] = jnp.zeros_like(AV)
     VE[:, 512:640] = jnp.ones((384, 128), BF16)
@@ -233,25 +256,23 @@
         PB[s] = (rr == target).astype(F32).astype(BF16)
 
     def st(k):
-        return rc(GM.at[role, pl.ds(384, 8)], ST.at[yr], s_st.at[k], r_st.at[k], (sib, yp, diag)[k])
+        return rc(GM.at[role, pl.ds(384, 8)], ST.at[yr], s_st.at[0], r_st.at[0], (sib, yp, diag)[k])
 
     def step(s):
-        zk(0, s, z - 1).wait_recv()
-        if s < 8:
-            zk(0, s + 1, z).start()
-        zk(1, s, z + 1).wait_recv()
-        if s < 8:
-            zk(1, s + 1, z).start()
+        for st in (2, 3, 0, 1):
+            for way in ways(st, s):
+                zc(st, way, s, (z - 1, z + 1)[way]).wait_recv()
+                if s < 8 and way in ways(st, s + 1):
+                    zc(st, way, s + 1, z).start()
+            if st == 3:
+                start(yv(s, yr))
         start(dk(s, c))
-        zv(0, s, z - 1, yr).wait_recv()
-        if s < 8:
-            zv(0, s + 1, z, yr).start()
-        zv(1, s, z + 1, yr).wait_recv()
-        if s < 8:
-            zv(1, s + 1, z, yr).start()
-        start(yv(s, yr))
-        wait_recv(yv(s - 1, yo))
-        start(dv(s - 1, c))
+        if s >= 2:
+            pass_on(s - 2)
+
+    def pass_on(s):
+        y_here(s)
+        start(dv(s, c))
 
     def token_step(s):
         if s <= 5:
@@ -259,7 +280,7 @@
             def _():
                 if s <= 4:
                     j = s - 1
-                    got = rc(tok(x, j), tok(x, j), s_sw.at[3 + j], r_sw.at[3 + j], partner)
+                    got = rc(tok(x, j), tok(x, j), s_sw.at[2], r_sw.at[3 + j], partner)
                     got.wait_recv()
                     t1(0, j, x).start()
                     t1(1, j, x).start()
@@ -285,8 +306,7 @@
     token_step(4)
     step(5)
     token_step(5)
-    for k in range(3):
-        st(k).wait_recv()
+    all_here(GM.at[0, pl.ds(0, 24)], r_st.at[0])
     mz, tz = [], []
     for s in range(2):
         later = jnp.zeros((1, 128), F32)
@@ -302,46 +322,41 @@
         mz.append(top)
         tz.append(later)
     step(6)
-    step(7)
-
-    @pl.when(swapped)
-    def _():
-        for j in range(4):
-            t2(0, j, wrap(x - 1, nx)).wait_recv()
-            t2(1, j, wrap(x + 1, nx)).wait_recv()
-
     def mm(b):
         xc = XB[role, :, :, pl.ds(pl.multiple_of(b * KR, KR), KR)].reshape(384, KR)
         r = pl.ds(pl.multiple_of(b * KR, KR), KR)
         AK[...] += jnp.dot(xc, WK[r, :], preferred_element_type=F32)
         AV[...] += jnp.dot(xc, WV[r, :], preferred_element_type=F32)
 
-    def wait_d(s):
-        wait_recv(dk(s, 1 - c))
-        wait_recv(dv(s, 1 - c))
-
     def mm_pair(s):
         def one(i, carry):
             mm(wrap(z + (2 * i - 1) * s, nz))
             return carry
         lax.fori_loop(0, 2, one, 0)
 
-    for s in range(6):
-        wait_d(s)
-
     def early(i, carry):
-        mm(wrap(z + i - 5, nz))
+        mm(wrap(z + i - 2, nz))
         return carry
 
-    lax.fori_loop(0, 11, early, 0)
+    @pl.when(swapped)
+    def _():
+        all_here(XB.at[1, :, :, pl.ds(0, 1024)], r_t2.at[0])
+
+    d_here(0)
+    lax.fori_loop(0, 5, early, 0)
+    step(7)
+    d_here(1)
+    mm_pair(3)
+    mm_pair(4)
     step(8)
-    wait_d(6)
+    pass_on(7)
+    d_here(2)
+    mm_pair(5)
     mm_pair(6)
-    wait_recv(yv(8, yo))
-    start(dv(8, c))
-    wait_d(7)
+    pass_on(8)
+    d_here(3)
     mm_pair(7)
-    wait_d(8)
+    d_here(4)
     mm(wrap(z + 8, nz))
 
     for s in range(2):
@@ -350,17 +365,63 @@
         KC[s * 192:(s + 1) * 192, :] = jnp.dot(kd, PB[s], preferred_element_type=F32).astype(BF16)
     VE[:, 0:512] = AV[...].astype(BF16)
 
-    def state(h):
-        cols = pl.ds(pl.multiple_of(h * 256, 256), 256)
-        out = lax.dot_general(KC[:, cols], VE[...], (((0,), (0,)), ((), ())), preferred_element_type=F32)
-        SF[cols, :] = out
-        SB[cols, :] = out.astype(BF16)
-
-    ys1 = rc(rows(SB, (1 - c) * 256, 256), R1, s_ys.at[0], r_ys.at[0], sib)
-    ys2 = rc(S2, R2, s_ys.at[1], r_ys.at[1], yp)
-    state(1 - c)
-    ys1.start()
-    state(c)
+    CUTS = (slice(0, 256), slice(256, 640))
+
+    def state(h, i):
+        half = pl.ds(pl.multiple_of(h * 256, 256), 256)
+        part = lax.dot_general(KC[:, half], VE[:, CUTS[i]], (((0,), (0,)), ((), ())), preferred_element_type=F32)
+        SF[half, CUTS[i]] = part
+        SB[half, CUTS[i]] = part.astype(BF16)
+
+    def ys1(i):
+        half = pl.ds(pl.multiple_of((1 - c) * 256, 256), 256)
+        w = pl.ds(CUTS[i].start, CUTS[i].stop - CUTS[i].start)
+        return rc(SB.at[half, w], R1.at[:, w], s_ys.at[0], r_ys.at[i], sib)
+
+    def ys2(i):
+        w = pl.ds(CUTS[i].start, CUTS[i].stop - CUTS[i].start)
+        return rc(S2.at[:, w], R2.at[:, w], s_ys.at[0], r_ys.at[2 + i], yp)
+
+    send_rows = pl.ds(pl.multiple_of(yo * 128, 128), 128)
+    keep_rows = pl.ds(pl.multiple_of(yr * 128, 128), 128)
+    send_part = pl.ds(pl.multiple_of((yo % 2) * 128, 128), 128)
+    keep_part = pl.ds(pl.multiple_of((yr % 2) * 128, 128), 128)
+
+    def pair_sum(i):
+        ys1(i).wait_recv()
+        S2[:, CUTS[i]] = (SF[send_rows, CUTS[i]] + R1[send_part, CUTS[i]].astype(F32)).astype(BF16)
+        ys2(i).start()
+
+    def kept(i):
+        ys2(i).wait_recv()
+        part = SF[keep_rows, CUTS[i]] + R1[keep_part, CUTS[i]].astype(F32) + R2[:, CUTS[i]].astype(F32)
+        return part.reshape(nz, 8, CUTS[i].stop - CUTS[i].start)
+
+    oy = jnp.where(swapped, 3 - y, y)
+    oc = jnp.where(swapped, 1 - c, c)
+
+    def zs(i, to):
+        return rc((MA, MB)[i].at[to], (RA, RB)[i].at[z], s_zs.at[i], r_zs.at[i], at(x, oy, to, oc))
+
+    def zsend(i):
+        for d in (8, 7, -7, 6, -6, 5, -5, 4, -4, 3, -3, 2, -2, 1, -1):
+            zs(i, wrap(z + d, nz)).start()
+
+        @pl.when(swapped)
+        def _():
+            zs(i, z).start()
+
+        @pl.when(native)
+        def _():
+            (RA, RB)[i][z] = (MA, MB)[i][z]
+
+    state(1 - c, 0)
+    ys1(0).start()
+    state(c, 0)
+    state(1 - c, 1)
+    ys1(1).start()
+    state(c, 1)
+    pair_sum(0)
     qsum = []
     sf_lo = (SF[...] - SB[...].astype(F32)).astype(BF16)
     for s in range(2):
@@ -378,20 +439,14 @@
     QM[8:16, :] = both[:, 512:640]
 
     def qm(k):
-        return rc(QM, QR.at[k], s_qm.at[k], r_qm.at[k], (sib, yp, diag)[k])
+        return rc(QM, QR.at[k], s_qm.at[0], r_qm.at[0], (sib, yp, diag)[k])
 
     for k in range(3):
         qm(k).start()
-    ys1.wait_recv()
-    send_rows = pl.ds(pl.multiple_of(yo * 128, 128), 128)
-    keep_rows = pl.ds(pl.multiple_of(yr * 128, 128), 128)
-    send_part = pl.ds(pl.multiple_of((yo % 2) * 128, 128), 128)
-    keep_part = pl.ds(pl.multiple_of((yr % 2) * 128, 128), 128)
-    S2[...] = (SF[send_rows, :] + R1[send_part, :].astype(F32)).astype(BF16)
-    ys2.start()
-    kept = SF[keep_rows, :] + R1[keep_part, :].astype(F32)
-    for k in range(3):
-        qm(k).wait_recv()
+    pair_sum(1)
+    MA[...] = kept(0).astype(BF16)
+    zsend(0)
+    all_here(GM.at[0, pl.ds(0, 48)], r_qm.at[0])
     qall = QM[...] + QR[0] + QR[1] + QR[2]
     qt, qn = qall[0:8], qall[8:16]
     lane8 = lax.broadcasted_iota(jnp.int32, (8, 128), 1)
@@ -401,44 +456,26 @@
     for base, v in ((2, m8), (5, t8), (8, qn)):
         for i, piece in enumerate(three(v)):
             head = jnp.where(lane8 == base + i, piece, head)
-    MB[:, :, 640:768] = jnp.broadcast_to(qt.astype(BF16)[None], (nz, 8, 128))
-    ys2.wait_recv()
-    kept = (kept + R2[...].astype(F32)).reshape(nz, 8, 640)
-    MB[:, :, 0:512] = kept[:, :, 0:512].astype(BF16)
-    norm = kept[:, :, 512:640]
+    MB[:, :, 384:512] = jnp.broadcast_to(qt.astype(BF16)[None], (nz, 8, 128))
+    part = kept(1)
+    MB[:, :, 0:256] = part[:, :, 0:256].astype(BF16)
+    norm = part[:, :, 256:384]
     norm_hi = norm.astype(BF16).astype(F32)
     lane3 = lax.broadcasted_iota(jnp.int32, (nz, 8, 128), 2)
     tail = jnp.where(lane3 == 0, norm_hi, jnp.where(lane3 == 1, norm - norm_hi, head[None]))
-    MB[:, :, 512:640] = tail.astype(BF16)
-
-    oy = jnp.where(swapped, 3 - y, y)
-    oc = jnp.where(swapped, 1 - c, c)
-
-    def zs(to):
-        return rc(MB.at[to], RB.at[z], s_zs.at[to], r_zs.at[z], at(x, oy, to, oc))
-
-    def zs_recv(frm):
-        return rc(MB.at[frm], RB.at[frm], s_zs.at[frm], r_zs.at[frm], at(x, oy, frm, oc))
-
-    for d in (8, 7, -7, 6, -6, 5, -5, 4, -4, 3, -3, 2, -2, 1, -1):
-        zs(wrap(z + d, nz)).start()
-
-    @pl.when(swapped)
-    def _():
-        zs(z).start()
-
-    @pl.when(native)
-    def _():
-        RB[z] = MB[z]
-
-    for d in (1, -1, 2, -2, 3, -3, 4, -4, 5, -5, 6, -6, 7, -7, 8):
-        zs_recv(wrap(z + d, nz)).wait_recv()
-
-    @pl.when(swapped)
-    def _():
-        zs_recv(z).wait_recv()
-
-    tails = RB[:, :, 512:640].astype(F32)
+    MB[:, :, 256:384] = tail.astype(BF16)
+    zsend(1)
+
+    for i in range(2):
+        @pl.when(native)
+        def _():
+            all_here((RA, RB)[i].at[pl.ds(0, nz - 1)], r_zs.at[i])
+
+        @pl.when(swapped)
+        def _():
+            all_here((RA, RB)[i], r_zs.at[i])
+
+    tails = RB[:, :, 256:384].astype(F32)
     m_all = jnp.sum(jnp.where((lane3 >= 2) & (lane3 < 5), tails, 0.0), axis=2, keepdims=True)
     t_all = jnp.sum(jnp.where((lane3 >= 5) & (lane3 < 8), tails, 0.0), axis=2, keepdims=True)
     later = jnp.zeros((8, 1), F32)
@@ -449,10 +486,13 @@
     top = lifts[0]
     for k in range(1, nz):
         top = jnp.maximum(top, lifts[k])
-    acc = jnp.zeros((8, 768), F32)
+    first = jnp.zeros((8, 256), F32)
+    acc = jnp.zeros((8, 512), F32)
     for k in range(nz):
-        acc = acc + jnp.exp(lifts[k] - top) * RB[k].astype(F32)
-    tail = acc[:, 512:640]
+        weight = jnp.exp(lifts[k] - top)
+        first = first + weight * RA[k].astype(F32)
+        acc = acc + weight * RB[k].astype(F32)
+    tail = acc[:, 256:384]
     norm = jnp.sum(jnp.where(lane8 < 2, tail, 0.0), axis=1, keepdims=True)
     qn = jnp.sum(jnp.where((lane8 >= 8) & (lane8 < 11), tail, 0.0), axis=1, keepdims=True)
     row1 = lax.broadcasted_iota(jnp.int32, (8, 1), 0)
@@ -467,40 +507,38 @@
     for s in range(2):
         for k in range(4):
             value = jnp.where(row8 == 4 * s + k, nv[s:s + 1, k * 128:(k + 1) * 128].astype(F32), value)
-    numer = carried * acc[:, 640:768] + fresh * own * value
+    numer = carried * acc[:, 384:512] + fresh * own * value
     denom = carried * qn + fresh * own
     read = numer / jnp.maximum(jnp.abs(denom), 1.0)
-    out[:, 0:512] = acc[:, 0:512]
+    out[:, 0:256] = first
+    out[:, 256:512] = acc[:, 0:256]
     out[:, 512:640] = jnp.where(lane8 == 0, top, norm)
     out[:, 640:768] = read
 
-    for s in range(1, 9):
-        for way in range(2):
-            zk(way, s, z).wait_send()
-            zv(way, s, z, yr).wait_send()
-    for s in range(9):
-        for cp in yv(s, yr) + dk(s, c) + dv(s, c):
-            cp.wait_send()
+    all_sent(rows(WK, 0, 1920), s_k.at[0])
+    all_sent(rows(WV, 0, 960), s_v.at[0])
+    all_sent(rows(WV, 0, 1024), s_y.at[0])
+    all_sent(rows(WV, 0, 3072), s_d.at[0])
     yk_send.wait_send()
-    for k in range(3):
-        st(k).wait_send()
-        qm(k).wait_send()
-    ys1.wait_send()
-    ys2.wait_send()
-    for d in range(1, 16):
-        zs(wrap(z + d - 16, nz)).wait_send()
+    all_sent(GM.at[0, pl.ds(0, 24)], s_st.at[0])
+    all_sent(GM.at[0, pl.ds(0, 48)], s_qm.at[0])
+    all_sent(rows(SB, 0, 384), s_ys.at[0])
+    for i in range(2):
+        @pl.when(native)
+        def _():
+            all_sent((MA, MB)[i].at[pl.ds(0, nz - 1)], s_zs.at[i])
+
+        @pl.when(swapped)
+        def _():
+            all_sent((MA, MB)[i], s_zs.at[i])
 
     @pl.when(swapped)
     def _():
-        zs(z).wait_send()
-        sw_v.wait_send()
-        sw_k.wait_send()
+        all_sent(rows(WV, 0, 96), s_sw.at[0])
         sw_g.wait_send()
-        for j in range(4):
-            sw_t(j).wait_send()
-            for way in range(2):
-                t1(way, j, x).wait_send()
-                t2(way, j, x).wait_send()
+        all_sent(XB.at[1, :, :, pl.ds(0, 1024)], s_sw.at[2])
+        all_sent(XB.at[1, :, :, pl.ds(0, 2048)], s_t.at[0])
+        all_sent(XB.at[1, :, :, pl.ds(0, 1024)], s_t.at[1])
 
 
 def unpack(got, o_mem, o_norm, o_max, o_read):
@@ -523,13 +561,12 @@
     nz = lax.axis_size("sp") // Y
     nx = lax.axis_size("tp") // 2
     vm = pl.BlockSpec(memory_space=pltpu.VMEM)
-    sm = pl.BlockSpec(memory_space=pltpu.SMEM)
     hb = pl.BlockSpec(memory_space=pltpu.HBM)
     dma = pltpu.SemaphoreType.DMA
     packed = pl.pallas_call(
         lambda *refs: kernel(nz, nx, *refs),
         out_shape=jax.ShapeDtypeStruct((8, 768), F32),
-        in_specs=[hb] * 5 + [sm] * 2 + [vm] * 4,
+        in_specs=[hb] * 11,
         out_specs=vm,
         scratch_shapes=[
             pltpu.VMEM((2, 2, 192, 4096), BF16),
@@ -552,23 +589,25 @@
             pltpu.VMEM((128, 640), BF16),
             pltpu.VMEM((16, 128), F32),
             pltpu.VMEM((3, 16, 128), F32),
-            pltpu.VMEM((nz, 8, 768), BF16),
-            pltpu.VMEM((nz, 8, 768), BF16),
-            dma((5,)),
-            dma((10, 9)), dma((10, 9)),
-            dma((1,)), dma((1,)),
-            dma((7,)), dma((7,)),
-            dma((4, 4)), dma((4, 4)),
-            dma((3,)), dma((3,)),
-            dma((3,)), dma((3,)),
-            dma((2,)), dma((2,)),
-            dma((nz,)), dma((nz,)),
+            pltpu.VMEM((nz, 8, 256), BF16),
+            pltpu.VMEM((nz, 8, 512), BF16),
+            pltpu.VMEM((nz, 8, 256), BF16),
+            pltpu.VMEM((nz, 8, 512), BF16),
+            pltpu.VMEM((1, 8), F32),
+            pltpu.VMEM((1, 8), F32),
+            pltpu.VMEM((2, 256), BF16),
+            pltpu.VMEM((2, 256), BF16),
+            pltpu.VMEM((2, 512), BF16),
+            pltpu.VMEM((2, 1, 2), F32),
+            dma((11,)), dma((1,)), dma((1,)), dma((1,)), dma((1,)), dma((60,)), dma((9,)), dma((5,)),
+            dma((1,)), dma((1,)), dma((3,)), dma((7,)), dma((2,)), dma((2, 4)), dma((1,)),
+            dma((1,)), dma((1,)), dma((1,)), dma((1,)), dma((1,)), dma((4,)), dma((2,)), dma((2,)),
         ],
         compiler_params=pltpu.CompilerParams(
             collective_id=0, has_side_effects=True, vmem_limit_bytes=56 * 1024 * 1024),
         name="prefill",
     )(
-        prompt, w_key, w_value, w_igate.T, w_fgate.T, input_bias, forget_bias,
+        prompt, w_key, w_value, w_igate.T, w_fgate.T, input_bias.reshape(1, 8), forget_bias.reshape(1, 8),
         new_query.reshape(2, 256), new_key.reshape(2, 256), new_value.reshape(2, 512),
         jnp.transpose(new_gates, (0, 2, 1)),
     )

time: 83.4 us -> 74.9 us (0.90)
  Pallas kernels: 82.6 us -> 74.1 us
    pallas_call x1, Pallas kernels: 81.2 us -> 72.7 us  [per_device(): pl.pallas_call(lambda *refs: kernel(nz, nx, *refs), out_shape=jax.ShapeDt...]
where the time goes in v3:
time: 74.9 us; the launch traced here: 74.7 us
  Pallas kernels  74.1 us (99%)
    pallas_call x1, Pallas kernels, per_device(): pl.pallas_call(lambda *refs: kernel(nz, nx, *refs), out_shape=jax.ShapeDt...  72.7 us

profile of v3, /device:TPU:1, one launch (start us, length us, event | category | flops | bytes accessed | tf_op | source)
XLA Modules:
  0.0 74.7 jit_solution(983134704869341428)
XLA Ops:
  0.6 72.7 %prefill.1.got = f32[8,768]{1,0:T(8,128)} custom-call(bf16[2,192,4096]{2,1,0:T(8,128)(2,1)} %refs_0_.1, bf16[64,256]{1,0:T(8,128)(2,1)} %refs_1_.1, bf16[64,512]{1,0:T(8,128)(2,1)} %refs_2_.1, bf16[8,4096]{1,0:T(8,128)(2,1)} %bitcast.12, bf16[8,4096]{1,0:T(8,128)(2,1)} %bitcast.13, f32[1,8]{1,0:T(1,128)} %bitcast.18, f32[1,8]{1,0:T(1,128)} %bitcast.19, ...), custom_call_target="tpu_custom_call" | custom-call | tf_op jit(solution)/shard_map/prefill/pallas_call | solution.py:566
  73.4 1.4 %unpack.1 = (bf16[2,1,4,512]{3,2,1,0:T(4,128)(2,1)}, f32[2,1,4]{2,1,0:T(1,128)}, f32[1,2]{1,0:T(1,128)}, bf16[2,512]{1,0:T(2,128)(2,1)}) custom-call(f32[8,768]{1,0:T(8,128)} %prefill.1.got), custom_call_target="tpu_custom_call" | custom-call | tf_op jit(solution)/shard_map/unpack/pallas_call | solution.py:614
